TPU v7x, 768 devices: a whole 4x8x12 slice. The times are simulated.
768 devices in a mesh: sp: 48 (over z, x), tp: 16 (over y, core).
Axes of the slice: x: 4, y: 8, z: 12, core: 2. Of those that a mesh axis runs over, the one named last changes fastest.
Arguments:
- tokens: bfloat16 [48, 480, 4096], P(None, 'sp', 'tp'), may hold values from -6 to 6
- latent_down_weight: bfloat16 [4096, 512], replicated, may hold values from -0.09375 to 0.09375
- w_rope_key: bfloat16 [4096, 64], replicated, may hold values from -0.09375 to 0.09375
- latent_norm_gain: float32 [512], replicated, may hold values from 0.1 to 1.9
- key_up_weight: bfloat16 [512, 4096], P(None, 'tp'), may hold values from -0.25 to 0.25
- value_up_weight: bfloat16 [512, 4096], P(None, 'tp'), may hold values from -0.25 to 0.25
- cached_latent_rows: bfloat16 [48, 32768, 512], P('sp', 'tp'), may hold values from -6 to 6
- past_rope: bfloat16 [48, 32768, 64], P('sp', 'tp'), may hold values from -6 to 6
- query_nope: bfloat16 [48, 4096], P('sp', 'tp'), may hold values from -8 to 8
- query_rope: bfloat16 [48, 2048], P('sp', 'tp'), may hold values from -300 to 300
Outputs:
- new_keys: bfloat16 [48, 480, 4096], P('sp', None, 'tp')
- new_values: bfloat16 [48, 480, 4096], P('sp', None, 'tp')
- new_rope: bfloat16 [48, 480, 64], P('sp')
- attended: bfloat16 [48, 4096], P('sp', 'tp')
All inputs are finite; a program needn't handle non-finite values.
Results may differ from a plain program's by a relative error of at most 0.0085.
Values may be sent and summed in bfloat16 or wider, within the bound.
No kernel may reach another device: no remote copies, remote signals or barrier semaphores. Data moves between devices by JAX's collectives and lax.ppermute only.
A program may use at most 64 MiB of HBM per device.

v0:
```python
import jax
import jax.numpy as jnp
from jax import lax
from jax.sharding import Mesh
from jax.sharding import PartitionSpec as P

PLAIN_KEY_WIDTH = 128
ROPE = 64
VALUE_WIDTH = 128
PAST_POSITIONS = 32768
TP = ("tp_0", "tp_1")


epsilon = 1e-06
rope_theta = 10000.0


def in_one_piece(arrays, axis, dim, along):
    ends, at = ([], 0)
    for a in arrays[:-1]:
        at += a.shape[along]
        ends.append(at)
    both = jnp.concatenate(arrays, axis=along)
    return tuple(jnp.split(lax.all_gather(both, axis, axis=dim, tiled=True), ends, axis=along))


def gathered_once(shard, axis):
    leaves = jax.tree.leaves(shard)
    turns = sorted(range(len(leaves)), key=lambda k: -leaves[k].size)
    width = (1, *leaves[turns[0]].shape)[-1]
    lines = [
        jnp.pad(leaves[k].reshape(-1), (0, -leaves[k].size % width)).reshape(-1, width)
        for k in turns
    ]
    both, at, found = (lax.all_gather(jnp.concatenate(lines), axis), 0, {})
    for k, line in zip(turns, lines):
        section = both[:, at : at + len(line)].reshape(len(both), -1)
        found[k] = section[:, : leaves[k].size].reshape(-1, *leaves[k].shape)
        at += len(line)
    numbers = iter(range(len(leaves)))
    return jax.tree.map(lambda _: found[next(numbers)], shard)


def merged_by_axis(shard, axes, combine):
    for axis in axes:
        pieces = gathered_once(shard, axis)
        shard = jax.tree.map(lambda part: part[0], pieces)
        for k in range(1, lax.axis_size(axis)):
            shard = combine(shard, jax.tree.map(lambda part: part[k], pieces))
    return shard


def rotate(values, positions):
    halfway = values.shape[-1] // 2
    frequency = rope_theta ** (-jnp.arange(halfway, dtype=jnp.float32) / halfway)
    angles = positions[:, None] * frequency
    first = values[..., :halfway]
    second = values[..., halfway:]
    return jnp.concatenate(
        [
            first * jnp.cos(angles) - second * jnp.sin(angles),
            first * jnp.sin(angles) + second * jnp.cos(angles),
        ],
        axis=-1,
    )


def combine_parts(first, second):
    highest = jnp.maximum(first[0], second[0])
    scale_first = jnp.exp(first[0] - highest)
    scale_second = jnp.exp(second[0] - highest)
    total = first[1] * scale_first + second[1] * scale_second
    summed = first[2] * scale_first[..., None] + second[2] * scale_second[..., None]
    return (highest, total, summed)


def on_device(
    tokens,
    latent_down_weight,
    w_rope_key,
    latent_norm_gain,
    key_up_weight,
    value_up_weight,
    cached_latent_rows,
    past_rope,
    query_nope,
    query_rope,
):
    rows_here = lax.all_to_all(tokens, "sp", split_axis=0, concat_axis=1, tiled=True)
    prompts, per_seq, features = rows_here.shape
    row_count = prompts * per_seq
    latent_width = latent_down_weight.shape[1]
    turn_width = w_rope_key.shape[1]
    factor = (PLAIN_KEY_WIDTH + ROPE) ** (-0.5)
    fragment = lax.all_gather(rows_here, TP, axis=2, tiled=True)
    columns = fragment.shape[2]
    flat_rows = fragment.reshape(row_count, columns)
    latent_raw = jnp.dot(flat_rows, latent_down_weight, preferred_element_type=jnp.float32)
    rope_raw = jnp.dot(flat_rows, w_rope_key, preferred_element_type=jnp.float32)
    scale = lax.rsqrt(jnp.mean(latent_raw * latent_raw, axis=-1, keepdims=True) + epsilon)
    latent = (latent_raw * scale * latent_norm_gain).astype(jnp.bfloat16)
    positions = (PAST_POSITIONS + jnp.arange(per_seq)).astype(jnp.float32)
    rope_local = rotate(rope_raw.reshape(prompts, per_seq, turn_width), positions).astype(
        jnp.bfloat16
    )
    keys_local = (
        jnp.dot(latent, key_up_weight, preferred_element_type=jnp.float32)
        .astype(jnp.bfloat16)
        .reshape(prompts, per_seq, key_up_weight.shape[1])
    )
    values_local = (
        jnp.dot(latent, value_up_weight, preferred_element_type=jnp.float32)
        .astype(jnp.bfloat16)
        .reshape(prompts, per_seq, value_up_weight.shape[1])
    )
    new_keys, new_values, new_rope = (keys_local, values_local, rope_local)
    owned = query_nope.shape[0]
    heads_local = query_nope.shape[1] // PLAIN_KEY_WIDTH
    query_own = query_nope.reshape(owned, heads_local, PLAIN_KEY_WIDTH)
    turn_own = query_rope.reshape(owned, heads_local, ROPE)
    head_keys = key_up_weight.reshape(latent_width, heads_local, PLAIN_KEY_WIDTH)
    query_latent = jnp.einsum(
        "shd,khd->shk", query_own, head_keys, preferred_element_type=jnp.float32
    ).astype(jnp.bfloat16)
    every_latent, every_turn = in_one_piece((query_latent, turn_own), TP, 1, 2)
    past_scores = jnp.einsum(
        "shk,spk->shp", every_latent, cached_latent_rows, preferred_element_type=jnp.float32
    )
    past_scores = (
        past_scores
        + jnp.einsum("shd,spd->shp", every_turn, past_rope, preferred_element_type=jnp.float32)
    ) * factor
    local_peak = jnp.max(past_scores, axis=-1)
    local_weight = jnp.exp(past_scores - local_peak[:, :, None])
    local_total = jnp.sum(local_weight, axis=-1)
    local_latent = jnp.einsum(
        "shp,spk->shk",
        local_weight.astype(jnp.bfloat16),
        cached_latent_rows,
        preferred_element_type=jnp.float32,
    )
    peak_all, total_all, latent_all = merged_by_axis(
        (local_peak, local_total, local_latent), TP, combine_parts
    )
    start = lax.axis_index(TP) * heads_local
    past_peak = lax.dynamic_slice_in_dim(peak_all, start, heads_local, 1)
    past_total = lax.dynamic_slice_in_dim(total_all, start, heads_local, 1)
    past_sum = lax.dynamic_slice_in_dim(latent_all, start, heads_local, 1)
    fresh = new_keys.shape[1]
    new_scores = jnp.einsum(
        "shd,sphd->shp",
        query_own,
        new_keys.reshape(owned, fresh, heads_local, PLAIN_KEY_WIDTH),
        preferred_element_type=jnp.float32,
    )
    new_scores = (
        new_scores
        + jnp.einsum("shd,spd->shp", turn_own, new_rope, preferred_element_type=jnp.float32)
    ) * factor
    peak = jnp.maximum(past_peak, jnp.max(new_scores, axis=-1))
    past_share = jnp.exp(past_peak - peak)
    new_weight = jnp.exp(new_scores - peak[:, :, None])
    denominator = past_total * past_share + jnp.sum(new_weight, axis=-1)
    latent_sum = (past_sum * past_share[..., None]).astype(jnp.bfloat16)
    head_values = value_up_weight.reshape(latent_width, heads_local, VALUE_WIDTH)
    past_out = jnp.einsum(
        "shk,khd->shd", latent_sum, head_values, preferred_element_type=jnp.float32
    )
    new_out = jnp.einsum(
        "shp,sphd->shd",
        new_weight.astype(jnp.bfloat16),
        new_values.reshape(owned, fresh, heads_local, VALUE_WIDTH),
        preferred_element_type=jnp.float32,
    )
    attended = (
        ((past_out + new_out) / denominator[:, :, None])
        .astype(jnp.bfloat16)
        .reshape(owned, heads_local * VALUE_WIDTH)
    )
    return (new_keys, new_values, new_rope, attended)


def solution(mesh):
    split = Mesh(mesh.devices.reshape(mesh.shape["sp"], 8, 2), ("sp", "tp_0", "tp_1"))
    return jax.shard_map(
        on_device,
        mesh=split,
        in_specs=(
            P(None, "sp", TP),
            P(),
            P(),
            P(),
            P(None, TP),
            P(None, TP),
            P("sp", TP, None),
            P("sp", TP, None),
            P("sp", TP),
            P("sp", TP),
        ),
        out_specs=(P("sp", None, TP), P("sp", None, TP), P("sp", None, None), P("sp", TP)),
        check_vma=False,
    )
```

profile of v0, /device:TPU:1, one launch (start us, length us, event | category | flops | bytes accessed | tf_op | source)
XLA Modules:
  0.0 120.5 jit_solution(15090978912912709654)
XLA Ops:
  7.2 0.0 copy-start
  7.2 0.0 all-gather.6.cloned.1.call-start
  7.2 1.2 copy.24
  8.4 38.8 %all_to_all.12 = bf16[48,10,256]{2,1,0:T(8,128)(2,1)S(1)} all-to-all(bf16[48,10,256]{2,1,0:T(8,128)(2,1)S(1)} %copy.24), channel_id=1, replica_groups=mesh['sp'=48,'tp_0'=8,'tp_1'=2] {'sp'}, dimensions={0} | all-to-all | bytes 491520 | tf_op jit(solution)/shard_map/all_to_all | solution.py:89
  47.3 0.8 all_to_all.10
  48.0 0.0 all-gather.6.cloned.1.call-update
  48.1 0.5 broadcast.212
  48.6 1.3 %reduce.13 = bf16[128]{0:T(256)(128)(2,1)S(1)} reduce(bf16[1,128]{1,0:T(2,128)(2,1)} %param.19, bf16[]{:T(256)} %broadcast.212), dimensions={0}, to_apply=%param.19.reduce_sub_computation.5 | reduce | bytes 514 | tf_op args[9]
  49.9 0.1 reshape.549
  50.0 1.1 fusion.17
  51.2 20.1 %all_gather.19 = bf16[1,32,576]{2,0,1:T(2,128)(2,1)S(1)} all-gather(bf16[1,2,576]{2,0,1:T(2,128)(2,1)S(1)} %copy.25), channel_id=1, replica_groups=mesh['sp'=48,'tp_0'=8,'tp_1'=2] {'tp_0','tp_1'}, dimensions={1}, use_global_device_ids=true | all-gather | bytes 39168 | tf_op jit(solution)/shard_map/all_gather | solution.py:24
  71.3 0.1 split.8
  71.4 0.7 reshape.565
  72.2 0.7 fusion.7
  72.9 0.3 fusion.112
  73.2 0.2 fusion.27
  73.4 0.5 fusion.5
  73.9 22.3 %all-gather.2 = f32[8,34,512]{2,1,0:T(8,128)S(1)} all-gather(f32[1,34,512]{2,1,0:T(8,128)S(1)} %maximum_bitcast_fusion), channel_id=2, replica_groups=mesh['sp'=48,'tp_0'=8,'tp_1'=2] {'tp_0'}, dimensions={0}, use_global_device_ids=true | all-gather | bytes 626688 | tf_op jit(solution)/shard_map/all_gather | solution.py:35
  96.4 0.1 fusion.40
  96.6 6.1 %all-gather.3 = f32[2,34,512]{2,1,0:T(8,128)S(1)} all-gather(f32[1,34,512]{2,1,0:T(8,128)S(1)} %maximum_bitcast_fusion.1), channel_id=3, replica_groups=mesh['sp'=48,'tp_0'=8,'tp_1'=2] {'tp_1'}, dimensions={0}, use_global_device_ids=true | all-gather | bytes 208896 | tf_op jit(solution)/shard_map/all_gather | solution.py:35
  102.7 0.1 dynamic-slice
  102.8 0.1 dynamic-slice.1
  102.9 0.0 copy-start.4
  102.9 0.0 copy-start.8
  102.9 0.0 copy-start.5
  102.9 0.0 copy-start.9
  102.9 0.0 copy-start.2
  103.0 0.0 all-gather.6.cloned.1.call-done
  103.0 0.0 copy-start.1
  103.0 5.8 %multiply_reduce_fusion = (f32[480]{0:T(512)S(1)}, f32[480,512]{1,0:T(8,128)S(1)}) fusion(bf16[4096,512]{1,0:T(8,128)(2,1)} %param.11, bf16[1,480,4096]{2,1,0:T(8,128)(2,1)} %all-gather.6.cloned.1.call-done), kind=kOutput, calls=%fused_computation.17 | convolution fusion | flops 2013756928 | bytes 9111424 | tf_op jit(solution)/shard_map/dot_general | solution.py:98
  108.8 0.3 convolution_convert_fusion.1
  109.2 0.0 copy-done.5
  109.2 0.0 copy-start.6
  109.2 0.3 convolution_convert_fusion
  109.6 0.0 copy-start.7
  109.6 0.2 fusion.24
  109.8 1.3 %fusion.9 = f32[1,480,64]{1,2,0:T(8,128)S(1)} fusion(bf16[4096,64]{0,1:T(8,128)(2,1)S(1)} %copy-done.2, bf16[1,480,4096]{2,1,0:T(8,128)(2,1)S(1)} %copy-done.1), kind=kOutput, calls=%fused_computation.12 | convolution fusion | flops 251658240 | bytes 4579328 | tf_op jit(solution)/shard_map/dot_general | solution.py:99
  111.1 0.3 fusion.36
  111.4 0.6 pad_maximum_fusion
  112.0 0.2 fusion.111
  112.3 0.1 fusion.88
  112.3 0.2 fusion.64
  112.5 0.1 fusion.106
  112.6 0.1 fusion.65
  112.7 0.2 fusion.14
  112.8 0.2 fusion.21
  113.0 0.1 fusion.86
  113.1 0.6 copy.91
  (37 shorter events, 0.3 us)
Async XLA Ops:
  7.2 65.0 %copy-start = (bf16[1,2048,512]{2,1,0:T(8,128)(2,1)S(1)}, bf16[1,2048,512]{2,1,0:T(8,128)(2,1)}, u32[]{:S(2)}) copy-start(bf16[1,2048,512]{2,1,0:T(8,128)(2,1)} %param.16) | copy-start | bytes 6291460
  7.2 65.7 %copy-start.3 = (bf16[1,2048,64]{1,2,0:T(8,128)(2,1)S(1)}, bf16[1,2048,64]{1,2,0:T(8,128)(2,1)}, u32[]{:S(2)}) copy-start(bf16[1,2048,64]{1,2,0:T(8,128)(2,1)} %param.17) | copy-start | bytes 786436
  7.2 95.8 %all-gather.6.cloned.1.call-start = ((), (), s32[]{:S(2)}) async-start(), calls=%async_computation.1 | async-start | bytes 4177920 | tf_op jit(solution)/shard_map/all_gather | solution.py:95
  102.9 5.9 %copy-start.4 = (bf16[512,256]{1,0:T(8,128)(2,1)S(1)}, bf16[512,256]{1,0:T(8,128)(2,1)}, u32[]{:S(2)}) copy-start(bf16[512,256]{1,0:T(8,128)(2,1)} %param.14) | copy-start | bytes 786436
  102.9 5.9 %copy-start.8 = (f32[512]{0:T(512)S(1)}, f32[512]{0:T(512)}, u32[]{:S(2)}) copy-start(f32[512]{0:T(512)} %param.13) | copy-start | bytes 6148
  102.9 6.3 %copy-start.5 = (bf16[512,256]{1,0:T(8,128)(2,1)S(1)}, bf16[512,256]{1,0:T(8,128)(2,1)}, u32[]{:S(2)}) copy-start(bf16[512,256]{1,0:T(8,128)(2,1)} %param.15) | copy-start | bytes 786436
  102.9 6.6 %copy-start.9 = (bf16[1,256]{1,0:T(2,128)(2,1)S(1)}, bf16[1,256]{1,0:T(2,128)(2,1)}, u32[]{:S(2)}) copy-start(bf16[1,256]{1,0:T(2,128)(2,1)} %param.18) | copy-start | bytes 1540
  102.9 6.8 %copy-start.2 = (bf16[4096,64]{0,1:T(8,128)(2,1)S(1)}, bf16[4096,64]{0,1:T(8,128)(2,1)}, u32[]{:S(2)}) copy-start(bf16[4096,64]{0,1:T(8,128)(2,1)} %param.12) | copy-start | bytes 1572868
  103.0 6.8 %copy-start.1 = (bf16[1,480,4096]{2,1,0:T(8,128)(2,1)S(1)}, bf16[1,480,4096]{2,1,0:T(8,128)(2,1)}, u32[]{:S(2)}) copy-start(bf16[1,480,4096]{2,1,0:T(8,128)(2,1)} %all-gather.6.cloned.1.call-done) | copy-start | bytes 11796484
  109.2 4.5 %copy-start.6 = (bf16[480,256]{1,0:T(8,128)(2,1)}, bf16[480,256]{1,0:T(8,128)(2,1)S(1)}, u32[]{:S(2)}) copy-start(bf16[480,256]{1,0:T(8,128)(2,1)S(1)} %convolution_convert_fusion.1) | copy-start | bytes 737284
  109.6 4.1 %copy-start.7 = (bf16[480,256]{1,0:T(8,128)(2,1)}, bf16[480,256]{1,0:T(8,128)(2,1)S(1)}, u32[]{:S(2)}) copy-start(bf16[480,256]{1,0:T(8,128)(2,1)S(1)} %convolution_convert_fusion) | copy-start | bytes 737284
Sparse Core Ops, SparseCore 0:
  48.2 52.6 all-gather.5
where the time goes:
time: 121 us
  blocking collectives  87.4 us (72%)
  between operations  14.3 us (12%)
  matrix products  11.1 us (9%)
  local copies, waits for them, and re-layouts  4.28 us (4%)
  other arithmetic  3.31 us (3%)
    all_to_all x1, blocking collectives, on_device(): lax.all_to_all(tokens, 'sp', split_axis=0, concat_axis=1, tiled=True)  38.8 us
    all_gather x2, blocking collectives, gathered_once(): both, at, found = (lax.all_gather(jnp.concatenate(lines), axis), 0, {})  28.4 us
    all_gather x1, blocking collectives, in_one_piece(): lax.all_gather(both, axis, axis=dim, tiled=True)  20.1 us
    dot_general x1, matrix products, on_device(): jnp.dot(flat_rows, latent_down_weight, preferred_element_type=jnp.float32)  5.8 us
  transfers between devices with their start and end apart: 1, of which 0 were waited for; matrix products, arithmetic and copies ran while one was open for 5% of the time, Pallas kernels for 0%

commit v1 on v0

v1 whole, which is shorter than its diff:
```python
import jax
import jax.numpy as jnp
from jax import lax
from jax.sharding import Mesh
from jax.sharding import PartitionSpec as P

PLAIN_KEY_WIDTH = 128
ROPE = 64
VALUE_WIDTH = 128
PAST_POSITIONS = 32768
TP = ("tp_0", "tp_1")
BLOCK = 32


epsilon = 1e-06
rope_theta = 10000.0


def rotate(values, positions):
    halfway = values.shape[-1] // 2
    frequency = rope_theta ** (-jnp.arange(halfway, dtype=jnp.float32) / halfway)
    angles = positions[:, None] * frequency
    first = values[..., :halfway]
    second = values[..., halfway:]
    return jnp.concatenate(
        [
            first * jnp.cos(angles) - second * jnp.sin(angles),
            first * jnp.sin(angles) + second * jnp.cos(angles),
        ],
        axis=-1,
    )


def split_parts(x, count):
    parts = []
    for _ in range(count - 1):
        part = lax.reduce_precision(x, 8, 7)
        parts.append(part.astype(jnp.bfloat16))
        x = x - part
    parts.append(x.astype(jnp.bfloat16))
    return parts


def on_device(
    tokens,
    latent_down_weight,
    w_rope_key,
    latent_norm_gain,
    key_up_weight,
    value_up_weight,
    cached_latent_rows,
    past_rope,
    query_nope,
    query_rope,
):
    f32, bf16 = jnp.float32, jnp.bfloat16
    factor = (PLAIN_KEY_WIDTH + ROPE) ** (-0.5)
    latent_width = latent_down_weight.shape[1]
    features = tokens.shape[2]
    heads = query_nope.shape[1] // PLAIN_KEY_WIDTH
    ranks = lax.axis_size(TP)
    pairs = lax.axis_size("tp_1")
    rings = ranks // pairs
    rank = lax.axis_index(TP)

    arrived = lax.all_to_all(tokens, "sp", split_axis=0, concat_axis=0, tiled=True)
    rows = arrived.reshape(-1, features)
    row_count = rows.shape[0]

    query_own = query_nope.reshape(heads, PLAIN_KEY_WIDTH)
    turn_own = query_rope.reshape(heads, ROPE)
    head_keys = key_up_weight.reshape(latent_width, heads, PLAIN_KEY_WIDTH)
    query_latent = jnp.einsum(
        "hd,khd->hk", query_own, head_keys, preferred_element_type=f32
    ).astype(bf16)

    latent_lines = heads * latent_width // features
    extra = 8
    query_lines = jnp.concatenate(
        [
            query_latent.reshape(latent_lines, features),
            jnp.pad(turn_own.reshape(1, -1), ((0, 0), (0, features - heads * ROPE))),
            jnp.zeros((extra - latent_lines - 1, features), bf16),
        ]
    )
    block = BLOCK
    workers = row_count // block
    blocks = jnp.pad(rows.reshape(workers, block, features), ((0, ranks - workers), (0, 0), (0, 0)))
    outgoing = jnp.concatenate(
        [blocks, jnp.broadcast_to(query_lines, (ranks, extra, features))], axis=1
    )
    whole = lax.all_to_all(outgoing, TP, split_axis=0, concat_axis=0, tiled=True)
    x = whole[:, :block].transpose(1, 0, 2).reshape(block, ranks * features)
    latent_raw = jnp.dot(x, latent_down_weight, preferred_element_type=f32)
    rope_raw = jnp.dot(x, w_rope_key, preferred_element_type=f32)
    scale = lax.rsqrt(jnp.mean(latent_raw * latent_raw, axis=-1, keepdims=True) + epsilon)
    latent_own = (latent_raw * scale * latent_norm_gain).astype(bf16)
    positions = (PAST_POSITIONS + rank * block + jnp.arange(block)).astype(f32)
    rope_own = rotate(rope_raw, positions).astype(bf16)

    every_latent = whole[:, block : block + latent_lines].reshape(ranks * heads, latent_width)
    every_turn = whole[:, block + latent_lines, : heads * ROPE].reshape(ranks * heads, ROPE)
    cached = cached_latent_rows[0]
    past_scores = jnp.einsum("hk,pk->hp", every_latent, cached, preferred_element_type=f32)
    past_scores = (
        past_scores + jnp.einsum("hd,pd->hp", every_turn, past_rope[0], preferred_element_type=f32)
    ) * factor
    local_peak = jnp.max(past_scores, axis=-1)
    local_weight = jnp.exp(past_scores - local_peak[:, None])
    local_total = jnp.sum(local_weight, axis=-1)
    local_latent = jnp.einsum(
        "hp,pk->hk", local_weight.astype(bf16), cached, preferred_element_type=f32
    )

    group = pairs * heads
    stats = jnp.stack(split_parts(local_peak, 3) + split_parts(local_total, 3))
    stats = stats.reshape(6, rings, group).transpose(1, 0, 2).reshape(rings, 1, 6 * group)
    stats = jnp.pad(stats, ((0, 0), (0, 0), (0, latent_width - 6 * group)))
    sums = [p.reshape(rings, group, latent_width) for p in split_parts(local_latent, 2)]
    turn_lines = block * ROPE // latent_width
    fixed = jnp.concatenate([latent_own, rope_own.reshape(turn_lines, latent_width)])
    chunk = jnp.concatenate(
        [jnp.broadcast_to(fixed, (rings, *fixed.shape)), *sums, stats], axis=1
    )
    chunk = jnp.pad(chunk, ((0, 0), (0, -chunk.shape[1] % 8), (0, 0)))
    got = lax.all_to_all(chunk, "tp_0", split_axis=0, concat_axis=0, tiled=True)
    both = lax.all_gather(got, "tp_1")

    ordered = both[:, :, : block + turn_lines].transpose(1, 0, 2, 3)
    ordered = ordered.reshape(ranks, block + turn_lines, latent_width)[:workers]
    latent = ordered[:, :block].reshape(row_count, latent_width)
    new_rope = ordered[:, block:].reshape(row_count, ROPE)
    at = block + turn_lines
    own = lax.axis_index("tp_1") * heads
    high = lax.dynamic_slice_in_dim(both[:, :, at : at + group], own, heads, 2)
    low = lax.dynamic_slice_in_dim(both[:, :, at + group : at + 2 * group], own, heads, 2)
    sums_all = high.astype(f32) + low.astype(f32)
    numbers = both[:, :, at + 2 * group, : 6 * group].reshape(pairs, rings, 6, group).astype(f32)
    numbers = lax.dynamic_slice_in_dim(numbers, own, heads, 3)
    peaks = numbers[:, :, 0] + numbers[:, :, 1] + numbers[:, :, 2]
    totals = numbers[:, :, 3] + numbers[:, :, 4] + numbers[:, :, 5]

    new_keys = jnp.dot(latent, key_up_weight, preferred_element_type=f32).astype(bf16)
    new_values = jnp.dot(latent, value_up_weight, preferred_element_type=f32).astype(bf16)

    new_scores = jnp.einsum(
        "hd,phd->hp",
        query_own,
        new_keys.reshape(row_count, heads, PLAIN_KEY_WIDTH),
        preferred_element_type=f32,
    )
    new_scores = (
        new_scores + jnp.einsum("hd,pd->hp", turn_own, new_rope, preferred_element_type=f32)
    ) * factor
    peak = jnp.maximum(jnp.max(peaks, axis=(0, 1)), jnp.max(new_scores, axis=-1))
    share = jnp.exp(peaks - peak)
    new_weight = jnp.exp(new_scores - peak[:, None])
    denominator = jnp.sum(totals * share, axis=(0, 1)) + jnp.sum(new_weight, axis=-1)
    latent_sum = jnp.sum(sums_all * share[..., None], axis=(0, 1)).astype(bf16)
    head_values = value_up_weight.reshape(latent_width, heads, VALUE_WIDTH)
    past_out = jnp.einsum("hk,khd->hd", latent_sum, head_values, preferred_element_type=f32)
    new_out = jnp.einsum(
        "hp,phd->hd",
        new_weight.astype(bf16),
        new_values.reshape(row_count, heads, VALUE_WIDTH),
        preferred_element_type=f32,
    )
    attended = ((past_out + new_out) / denominator[:, None]).astype(bf16).reshape(1, -1)
    return (new_keys[None], new_values[None], new_rope[None], attended)


def solution(mesh):
    split = Mesh(mesh.devices.reshape(mesh.shape["sp"], 8, 2), ("sp", "tp_0", "tp_1"))
    return jax.shard_map(
        on_device,
        mesh=split,
        in_specs=(
            P(None, "sp", TP),
            P(),
            P(),
            P(),
            P(None, TP),
            P(None, TP),
            P("sp", TP, None),
            P("sp", TP, None),
            P("sp", TP),
            P("sp", TP),
        ),
        out_specs=(P("sp", None, TP), P("sp", None, TP), P("sp", None, None), P("sp", TP)),
        check_vma=False,
    )
```

time: 121 us -> 105 us (0.87)
  blocking collectives: 87.4 us -> 2.38 us
  waiting for transfers between devices: 0.04 us -> 45 us
  starting transfers between devices: 0.04 us -> 31.9 us
  between operations: 14.3 us -> 0.98 us
  local copies, waits for them, and re-layouts: 4.28 us -> 11.3 us
  matrix products: 11.1 us -> 9.1 us
    all_gather x3 -> x1, blocking collectives: 48.5 us -> 2.38 us  [on_device(): both = lax.all_gather(got, 'tp_1')]
    all_to_all x0 -> x3, waiting for transfers between devices: none -> 45 us  [the longest x1 18.1 us: on_device(): lax.all_to_all(tokens, 'sp', split_axis=0, concat_axis=0, tiled=True)]
    all_to_all x1 -> x0, blocking collectives: 38.8 us -> none  [on_device(): lax.all_to_all(tokens, 'sp', split_axis=0, concat_axis=1, tiled=True)]
    all_to_all x0 -> x3, starting transfers between devices: none -> 31.9 us  [the longest x1 18.8 us: on_device(): lax.all_to_all(tokens, 'sp', split_axis=0, concat_axis=0, tiled=True)]
    unnamed x25 -> x26, local copies, waits for them, and re-layouts: 2.36 us -> 4.86 us
    reshape x2 -> x9, local copies, waits for them, and re-layouts: 0.09 us -> 2.26 us  [the longest x1 1.09 us: on_device(): head_keys = key_up_weight.reshape(latent_width, heads, PLAIN_KEY_WIDTH)]
    dot_general x12, matrix products: 11.1 us -> 9.1 us  [the longest x1 3.13 us: on_device(): latent_raw = jnp.dot(x, latent_down_weight, preferred_element_type=f32)]
  transfers between devices with their start and end apart: 1 -> 3, of which waited for: 0 -> 3; matrix products, arithmetic and copies ran while one was open for 5% -> 3% of each run, Pallas kernels for 0% -> 0%
where the time goes in v1:
time: 105 us; the launch traced here: 104 us
  waiting for transfers between devices  45 us (43%)
  starting transfers between devices  31.9 us (30%)
  local copies, waits for them, and re-layouts  11.3 us (11%)
  matrix products  9.1 us (9%)
  other arithmetic  3.76 us (4%)
  blocking collectives  2.38 us (2%)
    all_to_all x1, starting transfers between devices, on_device(): lax.all_to_all(tokens, 'sp', split_axis=0, concat_axis=0, tiled=True)  18.8 us
    all_to_all x1, waiting for transfers between devices, on_device(): lax.all_to_all(tokens, 'sp', split_axis=0, concat_axis=0, tiled=True)  18.1 us
    all_to_all x1, waiting for transfers between devices, on_device(): got = lax.all_to_all(chunk, 'tp_0', split_axis=0, concat_axis=0, tiled=True)  13.9 us
    all_to_all x1, waiting for transfers between devices, on_device(): lax.all_to_all(outgoing, TP, split_axis=0, concat_axis=0, tiled=True)  12.9 us
    all_to_all x1, starting transfers between devices, on_device(): lax.all_to_all(outgoing, TP, split_axis=0, concat_axis=0, tiled=True)  9.62 us
    unnamed x26, local copies, waits for them, and re-layouts  4.86 us
    all_to_all x1, starting transfers between devices, on_device(): got = lax.all_to_all(chunk, 'tp_0', split_axis=0, concat_axis=0, tiled=True)  3.45 us
    dot_general x1, matrix products, on_device(): latent_raw = jnp.dot(x, latent_down_weight, preferred_element_type=f32)  3.13 us
  transfers between devices with their start and end apart: 3, of which 3 were waited for; matrix products, arithmetic and copies ran while one was open for 3% of the time, Pallas kernels for 0%

profile of v1, /device:TPU:1, one launch (start us, length us, event | category | flops | bytes accessed | tf_op | source)
XLA Modules:
  0.0 104.4 jit_solution(11491094297393264500)
XLA Ops:
  0.7 1.9 %copy.46 = bf16[48,10,256]{2,1,0:T(8,128)(2,1)} copy(bf16[48,10,256]{2,0,1:T(8,128)(2,1)} %param.10) | data formatting | bytes 491520 | tf_op args[0]
  2.6 18.8 %all-to-all-start = ((bf16[48,10,256]{2,1,0:T(8,128)(2,1)}), bf16[48,10,256]{2,1,0:T(8,128)(2,1)S(1)}, u32[]{:S(2)}, u32[]{:S(2)}) async-start(bf16[48,10,256]{2,1,0:T(8,128)(2,1)} %copy.46), calls=%async_computation | async-start | bytes 786432 | tf_op jit(solution)/shard_map/all_to_all | solution.py:66
  21.4 1.1 %copy.69 = bf16[512,256]{0,1:T(8,128)(2,1)S(1)} copy(bf16[512,256]{1,0:T(8,128)(2,1)} %param.14) | data formatting | bytes 524288 | tf_op jit(solution)/shard_map/reshape | solution.py:72
  22.5 0.8 fusion.50
  23.5 18.1 %all-to-all-done = bf16[48,10,256]{2,1,0:T(8,128)(2,1)S(1)} async-done(((bf16[48,10,256]{2,1,0:T(8,128)(2,1)}), bf16[48,10,256]{2,1,0:T(8,128)(2,1)S(1)}, u32[]{:S(2)}, u32[]{:S(2)}) %all-to-all-start) | async-done | bytes 245792 | tf_op jit(solution)/shard_map/all_to_all | solution.py:66
  41.6 0.1 reshape_reshape.3
  41.7 0.7 fusion.10
  42.5 9.6 %all-to-all-start.1 = ((bf16[16,40,256]{2,1,0:T(8,128)(2,1)}), bf16[16,40,256]{2,1,0:T(8,128)(2,1)S(1)}, u32[]{:S(2)}, u32[]{:S(2)}) async-start(bf16[16,40,256]{2,1,0:T(8,128)(2,1)} %fusion.10), calls=%async_computation.1 | async-start | bytes 655360 | tf_op jit(solution)/shard_map/all_to_all | solution.py:92
  52.1 12.9 %all-to-all-done.1 = bf16[16,40,256]{2,1,0:T(8,128)(2,1)S(1)} async-done(((bf16[16,40,256]{2,1,0:T(8,128)(2,1)}), bf16[16,40,256]{2,1,0:T(8,128)(2,1)S(1)}, u32[]{:S(2)}, u32[]{:S(2)}) %all-to-all-start.1) | async-done | bytes 327712 | tf_op jit(solution)/shard_map/all_to_all | solution.py:92
  65.1 0.1 reshape_squeeze.4
  65.2 0.7 fusion.3
  66.0 0.3 fusion.57
  66.2 0.2 fusion.21
  66.5 0.5 reduce-precision_convert_fusion
  67.2 0.3 fusion.59
  67.4 3.1 %multiply_reduce_fusion.1 = (f32[32]{0:T(128)S(1)}, f32[32,512]{1,0:T(8,128)S(1)}) fusion(bf16[32,4096]{1,0:T(8,128)(2,1)S(1)} %bitcast.110, bf16[4096,512]{1,0:T(8,128)(2,1)} %param.11), kind=kOutput, calls=%fused_computation.38 | convolution fusion | flops 134250464 | bytes 4522112 | tf_op jit(solution)/shard_map/dot_general | solution.py:94
  70.6 0.1 fusion.31
  70.7 0.1 pad_maximum_fusion.1
  70.8 0.1 convert_element_type.131
  71.1 0.1 copy.48
  71.2 0.1 copy.71
  71.4 0.1 fusion.9
  71.5 0.8 pad.19
  72.3 3.5 %all-to-all-start.2 = ((bf16[8,48,512]{2,1,0:T(8,128)(2,1)}), bf16[8,48,512]{2,1,0:T(8,128)(2,1)S(1)}, u32[]{:S(2)}, u32[]{:S(2)}) async-start(bf16[8,48,512]{2,1,0:T(8,128)(2,1)} %pad.19), calls=%async_computation.2 | async-start | bytes 786432 | tf_op jit(solution)/shard_map/all_to_all | solution.py:126
  75.8 0.5 broadcast.58
  76.3 0.7 reduce.6
  76.9 0.1 reshape.232
  77.0 13.9 %all-to-all-done.2 = bf16[8,48,512]{2,1,0:T(8,128)(2,1)S(1)} async-done(((bf16[8,48,512]{2,1,0:T(8,128)(2,1)}), bf16[8,48,512]{2,1,0:T(8,128)(2,1)S(1)}, u32[]{:S(2)}, u32[]{:S(2)}) %all-to-all-start.2) | async-done | bytes 393248 | tf_op jit(solution)/shard_map/all_to_all | solution.py:126
  90.9 2.4 %all-gather = bf16[16,48,512]{2,1,0:T(8,128)(2,1)S(1)} all-gather(bf16[8,48,512]{2,1,0:T(8,128)(2,1)S(1)} %all-to-all-done.2), channel_id=2, replica_groups=mesh['sp'=48,'tp_0'=8,'tp_1'=2] {'tp_1'}, dimensions={0}, use_global_device_ids=true | all-gather | bytes 1179648 | tf_op jit(solution)/shard_map/all_gather | solution.py:127
  93.3 0.7 fusion.56
  94.1 0.6 copy.50
  94.7 0.2 reshape.228
  95.1 0.8 reshape.231
  95.9 0.8 broadcast_in_dim_reshape.3
  96.7 0.3 copy.51
  97.0 1.7 %copy.57 = bf16[1,480,64]{1,2,0:T(8,128)(2,1)} copy(bf16[1,480,64]{2,1,0:T(8,128)(2,1)} %broadcast_in_dim_reshape.3) | data formatting | bytes 122880
  98.7 0.3 convolution_convert_fusion.1
  99.0 1.3 %convolution_convert_fusion = bf16[480,256]{1,0:T(8,128)(2,1)S(1)} fusion(bf16[480,512]{1,0:T(8,128)(2,1)S(1)} %bitcast.105, bf16[512,256]{1,0:T(8,128)(2,1)} %param.15), kind=kOutput, calls=%fused_computation.6 | convolution fusion | flops 125952000 | bytes 999424 | tf_op jit(solution)/shard_map/dot_general | solution.py:144
  100.4 0.2 fusion.18
  100.6 0.3 fusion.58
  100.9 0.1 fusion.55
  101.0 0.2 fusion.47
  101.2 0.2 fusion.48
  101.4 0.1 copy.56
  101.5 1.0 multiply_reduce_fusion
  102.5 1.1 %fusion.11 = f32[2,1,128]{2,1,0:T(1,128)S(1)} fusion(bf16[2,512,1]{1,0,2:T(2,128)(2,1)S(1)} %bitcast.119, bf16[512,256]{1,0:T(8,128)(2,1)} %param.15), kind=kOutput, calls=%fused_computation.18 | convolution fusion | flops 262144 | bytes 265216 | tf_op jit(solution)/shard_map/hk,khd->hd/dot_general | solution.py:161
  103.6 0.2 fusion.15
  103.8 0.6 copy.98
  (57 shorter events, 1.1 us)
Async XLA Ops:
  0.6 64.6 %copy-start = (bf16[1,2048,512]{2,1,0:T(8,128)(2,1)S(1)}, bf16[1,2048,512]{2,1,0:T(8,128)(2,1)}, u32[]{:S(2)}) copy-start(bf16[1,2048,512]{2,1,0:T(8,128)(2,1)} %param.16) | copy-start | bytes 6291460
  0.6 22.8 %copy-start.9 = (bf16[1,128]{1,0:T(2,128)(2,1)S(1)}, bf16[1,128]{1,0:T(2,128)(2,1)}, u32[]{:S(2)}) copy-start(bf16[1,128]{1,0:T(2,128)(2,1)} %param.19) | copy-start | bytes 772
  2.6 39.0 %all-to-all-start = ((bf16[48,10,256]{2,1,0:T(8,128)(2,1)}), bf16[48,10,256]{2,1,0:T(8,128)(2,1)S(1)}, u32[]{:S(2)}, u32[]{:S(2)}) async-start(bf16[48,10,256]{2,1,0:T(8,128)(2,1)} %copy.46), calls=%async_computation | async-start | bytes 786432 | tf_op jit(solution)/shard_map/all_to_all | solution.py:66
  41.7 24.2 %copy-start.4 = (bf16[1,2048,64]{1,2,0:T(8,128)(2,1)S(1)}, bf16[1,2048,64]{1,2,0:T(8,128)(2,1)}, u32[]{:S(2)}) copy-start(bf16[1,2048,64]{1,2,0:T(8,128)(2,1)} %param.17) | copy-start | bytes 786436
  42.5 22.6 %all-to-all-start.1 = ((bf16[16,40,256]{2,1,0:T(8,128)(2,1)}), bf16[16,40,256]{2,1,0:T(8,128)(2,1)S(1)}, u32[]{:S(2)}, u32[]{:S(2)}) async-start(bf16[16,40,256]{2,1,0:T(8,128)(2,1)} %fusion.10), calls=%async_computation.1 | async-start | bytes 655360 | tf_op jit(solution)/shard_map/all_to_all | solution.py:92
  65.9 1.2 %copy-start.2 = (bf16[4096,64]{0,1:T(8,128)(2,1)S(1)}, bf16[4096,64]{0,1:T(8,128)(2,1)}, u32[]{:S(2)}) copy-start(bf16[4096,64]{0,1:T(8,128)(2,1)} %param.12) | copy-start | bytes 1572868
  67.4 3.9 %copy-start.7 = (f32[512]{0:T(512)S(1)}, f32[512]{0:T(512)}, u32[]{:S(2)}) copy-start(f32[512]{0:T(512)} %param.13) | copy-start | bytes 6148
  72.3 18.7 %all-to-all-start.2 = ((bf16[8,48,512]{2,1,0:T(8,128)(2,1)}), bf16[8,48,512]{2,1,0:T(8,128)(2,1)S(1)}, u32[]{:S(2)}, u32[]{:S(2)}) async-start(bf16[8,48,512]{2,1,0:T(8,128)(2,1)} %pad.19), calls=%async_computation.2 | async-start | bytes 786432 | tf_op jit(solution)/shard_map/all_to_all | solution.py:126
  94.7 4.0 %copy-start.1 = (bf16[512,256]{1,0:T(8,128)(2,1)S(1)}, bf16[512,256]{1,0:T(8,128)(2,1)}, u32[]{:S(2)}) copy-start(bf16[512,256]{1,0:T(8,128)(2,1)} %param.14) | copy-start | bytes 786436
  95.0 5.3 %copy-start.8 = (bf16[1,256]{1,0:T(2,128)(2,1)S(1)}, bf16[1,256]{1,0:T(2,128)(2,1)}, u32[]{:S(2)}) copy-start(bf16[1,256]{1,0:T(2,128)(2,1)} %param.18) | copy-start | bytes 1540
  97.0 3.5 %copy-start.3 = (bf16[480,64]{1,0:T(8,128)(2,1)S(1)}, bf16[480,64]{1,0:T(8,128)(2,1)}, u32[]{:S(2)}) copy-start(bf16[480,64]{1,0:T(8,128)(2,1)} %reshape.231) | copy-start | bytes 184324
  99.0 5.4 %copy-start.5 = (bf16[480,256]{1,0:T(8,128)(2,1)}, bf16[480,256]{1,0:T(8,128)(2,1)S(1)}, u32[]{:S(2)}) copy-start(bf16[480,256]{1,0:T(8,128)(2,1)S(1)} %convolution_convert_fusion.1) | copy-start | bytes 737284
  100.3 4.1 %copy-start.6 = (bf16[480,256]{1,0:T(8,128)(2,1)}, bf16[480,256]{1,0:T(8,128)(2,1)S(1)}, u32[]{:S(2)}) copy-start(bf16[480,256]{1,0:T(8,128)(2,1)S(1)} %convolution_convert_fusion) | copy-start | bytes 737284
